TPU v7x, 32 devices: a whole 2x2x4 slice. The times are simulated.
32 devices in a mesh: grp: 2 (over y), sp: 4 (over z), tp: 4 (over x, core).
Axes of the slice: x: 2, y: 2, z: 4, core: 2. Of those that a mesh axis runs over, the one named last changes fastest.
Arguments:
- queries: bfloat16 [2048, 512], P(('grp', 'sp'), 'tp'), parts along dimension 0, may hold values from -6 to 6
- key_rows: bfloat16 [2048, 512], P(('grp', 'sp'), 'tp'), parts along dimension 0, may hold values from -6 to 6
- value_rows: bfloat16 [2048, 1024], P(('grp', 'sp'), 'tp'), parts along dimension 0, may hold values from -6 to 6
- out_gate: bfloat16 [2048, 1024], P(('grp', 'sp'), 'tp'), parts along dimension 0, may hold values from -6 to 6
- log_decay: float32 [2, 2048, 512], P(None, ('grp', 'sp'), 'tp'), parts along dimension 1
- doc_ids: int32 [2048], P(('grp', 'sp')), parts along dimension 0, may hold values from 0 to 1, as said below
- head_gain: float32 [1024], P('tp'), may hold values from 0.1 to 1.9
- out_weight: bfloat16 [1024, 2048], P('tp'), may hold values from -0.375 to 0.375
- residual: bfloat16 [2048, 2048], P(('grp', 'sp'), 'tp'), parts along dimension 0
- norm_gain: float32 [2, 2048], replicated, may hold values from 0.1 to 1.9
- norm_bias: float32 [2, 2048], replicated, may hold values from -3 to 3
- gate_weight: bfloat16 [2048, 3072], P('sp', 'tp'), may hold values from -0.125 to 0.125
- up_weight: bfloat16 [2048, 3072], P('sp', 'tp'), may hold values from -0.125 to 0.125
- down_weight: bfloat16 [3072, 2048], P('tp', 'sp'), may hold values from -0.109375 to 0.109375
Outputs:
- layer_out: bfloat16 [2048, 2048], P(('grp', 'sp'), 'tp'), parts along dimension 0
There are 2 independent parts, one for each index of `grp`. A program takes and returns all parts, laid end to end along the dimension named above; an argument that names none is the same for every part. Nothing has to cross between parts.
Inputs may be any that keep to these rules, and one draw needn't show every extreme that they name: `doc_ids`: document numbers start at 0 and never fall; they rise by one at each of 1 positions, the k-th rise lying within half of 256 positions of k times 1024 divided by 2.
All inputs are finite; a program needn't handle non-finite values.
Results may differ from a plain program's by a relative error of at most 0.009.
Values may be sent and summed in bfloat16 or wider, within the bound.
A program may use at most 128 MiB of HBM per device.

v0:
```python
import jax
import jax.numpy as jnp
from jax import lax
from jax.sharding import PartitionSpec as P

DK = 32
DV = 64
BLOCK = 64


EPS = 1e-06
HIGH = lax.Precision.HIGHEST


def entering(x, axis, combine, identity, reverse):
    peers, position = (lax.axis_size(axis), lax.axis_index(axis))
    everything = jax.tree.map(
        lambda part, kind: lax.all_gather(part.astype(kind), axis),
        x,
        jax.tree.map(lambda a: jnp.bfloat16 if a.dtype == jnp.float32 else a.dtype, x),
    )
    start = jax.tree.map(
        lambda part, zero: jnp.broadcast_to(jnp.asarray(zero, part.dtype), part.shape), x, identity
    )

    def hop(k, before):
        at = peers - 1 - k if reverse else k
        reached = at > position if reverse else at < position
        new = combine(
            before, jax.tree.map(lambda part, own: part[at].astype(own.dtype), everything, x)
        )
        return jax.tree.map(lambda a, b: jnp.where(reached, a, b), new, before)

    return lax.fori_loop(0, peers, hop, start)


def run_blocks(query, key_part, value_part, decay, docs):
    length = query.shape[0]
    count = length // BLOCK
    head_count = query.shape[1]
    lower = jnp.arange(BLOCK)[:, None] >= jnp.arange(BLOCK)[None, :]

    def blocked(array):
        return array.reshape((count, BLOCK) + array.shape[1:])

    def advance(carried, inputs):
        state, state_doc = carried
        query_block, key_block, value_block, decay_block, doc_block = inputs
        running = jnp.cumsum(decay_block, axis=0)
        allowed = lower & (doc_block[:, None] == doc_block[None, :])
        relative = jnp.exp(
            jnp.where(allowed[:, :, None, None], running[:, None] - running[None, :], -jnp.inf)
        )
        scores = jnp.einsum("ihd,jhd,ijhd->hij", query_block, key_block, relative, precision=HIGH)
        within = jnp.einsum("hij,jhe->ihe", scores, value_block, precision=HIGH)
        linked = (doc_block == state_doc).astype(jnp.float32)
        carried_part = (
            jnp.einsum("ihd,hde->ihe", query_block * jnp.exp(running), state, precision=HIGH)
            * linked[:, None, None]
        )
        closing = doc_block[-1]
        ending = (doc_block == closing).astype(jnp.float32)
        tail_decay = jnp.exp(running[-1][None] - running) * ending[:, None, None]
        kept = (state_doc == closing).astype(jnp.float32)
        state = kept * jnp.exp(running[-1])[:, :, None] * state + jnp.einsum(
            "jhd,jhe->hde", key_block * tail_decay, value_block, precision=HIGH
        )
        return ((state, closing), within + carried_part)

    start = (
        jnp.zeros((head_count, query.shape[2], value_part.shape[2]), jnp.float32),
        jnp.array(-1, jnp.int32),
    )
    (state, closing), outputs = lax.scan(
        advance,
        start,
        tuple((blocked(array) for array in (query, key_part, value_part, decay, docs))),
    )
    return (outputs.reshape(length, head_count, value_part.shape[2]), state, closing)


def chain(earlier, later):
    early_state, early_pass, early_entry, early_leave = earlier
    late_state, late_pass, late_entry, late_leave = later
    joined = (late_entry == early_leave) | (early_leave < 0.0) | (late_entry < 0.0)
    keep = jnp.where(joined, jnp.float32(1.0), jnp.float32(0.0))
    state = late_state + keep * late_pass[:, :, None] * early_state
    passing = keep * early_pass * late_pass
    entry = jnp.where(early_entry < 0.0, late_entry, early_entry)
    leaving = jnp.where(late_leave < 0.0, early_leave, late_leave)
    return (state, passing, entry, leaving)


def one_way(query, key_part, value_part, decay, docs, backward):
    local_out, state, closing = run_blocks(query, key_part, value_part, decay, docs)
    passing = jnp.exp(jnp.sum(decay, axis=0)) * (docs[0] == closing).astype(jnp.float32)
    piece = (state, passing, docs[0].astype(jnp.float32), closing.astype(jnp.float32))
    identity = (jnp.zeros_like(state), jnp.ones_like(passing), jnp.float32(-1.0), jnp.float32(-1.0))
    if backward:
        carried = entering(piece, "sp", chain, identity, True)
    else:
        carried = entering(piece, "sp", chain, identity, False)
    incoming, _, _, leaving = carried
    linked = (docs.astype(jnp.float32) == leaving).astype(jnp.float32)
    reach = query * jnp.exp(jnp.cumsum(decay, axis=0))
    return (
        local_out
        + jnp.einsum("ihd,hde->ihe", reach, incoming, precision=HIGH) * linked[:, None, None]
    )


def apply_norm(stream, moments, full_width, gain, bias):
    middle = moments[0][:, None] / full_width
    spread = moments[1][:, None] / full_width - middle * middle
    return (stream - middle) * lax.rsqrt(spread + EPS) * gain + bias


def on_device(
    queries,
    key_rows,
    value_rows,
    out_gate,
    log_decay,
    doc_ids,
    head_gain,
    out_weight,
    residual,
    norm_gain,
    norm_bias,
    gate_weight,
    up_weight,
    down_weight,
):
    collected = None
    length = queries.shape[0]
    head_count = queries.shape[1] // DK
    query = queries.astype(jnp.float32).reshape(length, head_count, DK) * DK ** (-0.5)
    key_part = key_rows.astype(jnp.float32).reshape(length, head_count, DK)
    value_part = value_rows.astype(jnp.float32).reshape(length, head_count, DV)
    forward_decay = log_decay[0].reshape(length, head_count, DK)
    backward_decay = log_decay[1].reshape(length, head_count, DK)
    forward_out = one_way(query, key_part, value_part, forward_decay, doc_ids, False)
    backward_out = one_way(
        query[::-1], key_part[::-1], value_part[::-1], backward_decay[::-1], doc_ids[::-1], True
    )[::-1]
    attended = forward_out + backward_out
    normed = attended * lax.rsqrt(jnp.mean(attended * attended, axis=-1, keepdims=True) + EPS)
    mixed = (
        normed.reshape(length, -1) * head_gain * jax.nn.silu(out_gate.astype(jnp.float32))
    ).astype(jnp.bfloat16)
    partial_value = jnp.dot(mixed, out_weight, preferred_element_type=jnp.float32)
    collected = (
        lax.all_gather(gate_weight, "sp", axis=0, tiled=True),
        lax.all_gather(up_weight, "sp", axis=0, tiled=True),
        lax.all_gather(down_weight, "sp", axis=1, tiled=True),
    )
    gate_full, up_full, down_full = collected
    own_width = residual.shape[1]
    full_width = own_width * lax.axis_size("tp")
    offset = lax.axis_index("tp") * own_width
    branch = lax.psum_scatter(
        partial_value.astype(jnp.bfloat16), "tp", scatter_dimension=1, tiled=True
    ).astype(jnp.float32)
    stream = residual.astype(jnp.float32) + branch
    moments = lax.psum((jnp.sum(stream, axis=1), jnp.sum(stream * stream, axis=1)), "tp")
    settled = apply_norm(
        stream,
        moments,
        full_width,
        lax.dynamic_slice_in_dim(norm_gain[0], offset, own_width, 0),
        lax.dynamic_slice_in_dim(norm_bias[0], offset, own_width, 0),
    )
    features = settled.astype(jnp.bfloat16)
    piece = lax.all_gather(features, "tp", axis=1, tiled=True)
    gate = jnp.dot(piece, gate_full, preferred_element_type=jnp.float32)
    up_part = jnp.dot(piece, up_full, preferred_element_type=jnp.float32)
    inner = (jax.nn.silu(gate) * up_part).astype(jnp.bfloat16)
    down = lax.psum_scatter(
        jnp.dot(inner, down_full, preferred_element_type=jnp.float32).astype(jnp.bfloat16),
        "tp",
        scatter_dimension=1,
        tiled=True,
    ).astype(jnp.float32)
    final = settled + 0.5 * down
    closing_moments = lax.psum((jnp.sum(final, axis=1), jnp.sum(final * final, axis=1)), "tp")
    result = apply_norm(
        final,
        closing_moments,
        full_width,
        lax.dynamic_slice_in_dim(norm_gain[1], offset, own_width, 0),
        lax.dynamic_slice_in_dim(norm_bias[1], offset, own_width, 0),
    )
    return result.astype(jnp.bfloat16)


def solution(mesh):
    in_specs = (
        P(("grp", "sp"), "tp"),
        P(("grp", "sp"), "tp"),
        P(("grp", "sp"), "tp"),
        P(("grp", "sp"), "tp"),
        P(None, ("grp", "sp"), "tp"),
        P(("grp", "sp")),
        P("tp"),
        P("tp", None),
        P(("grp", "sp"), "tp"),
        P(),
        P(),
        P("sp", "tp"),
        P("sp", "tp"),
        P("tp", "sp"),
    )
    out_specs = P(("grp", "sp"), "tp")
    return jax.shard_map(
        on_device, mesh=mesh, in_specs=in_specs, out_specs=out_specs, check_vma=False
    )
```

profile of v0, /device:TPU:0, one launch (start us, length us, event | category | flops | bytes accessed | tf_op | source)
XLA Modules:
  0.0 599.7 jit_solution(14972712356723388708)
XLA Ops:
  20.4 91.4 %while.66 = (s32[]{:T(128)}, f32[4,32,64]{2,1,0:T(8,128)S(1)}, s32[]{:T(128)}, f32[4,64,4,64]{1,0,3,2:T(4,128)}, s32[4,64]{1,0:T(4,128)S(1)}, /*index=5*/f32[4,6...) while((s32[]{:T(128)}, f32[4,32,64]{2,1,0:T(8,128)S(1)}, ...), condition=%wide.region_10.11_spmd.clone, body=%wide.region_8.10_spmd.clone.sunk | while | flops 28397956 | bytes 10073782 | solution.py:74
  24.7 5.8 copy.268
  37.0 4.5 dynamic_update_slice.12
  47.6 5.8 copy.268
  59.8 4.5 dynamic_update_slice.12
  70.5 5.8 copy.268
  82.7 4.5 dynamic_update_slice.12
  93.3 5.8 copy.268
  105.6 4.5 dynamic_update_slice.12
  117.5 88.7 %while.64 = (s32[]{:T(128)}, f32[4,32,64]{2,1,0:T(8,128)S(1)}, s32[]{:T(128)}, f32[4,64,4,64]{1,0,3,2:T(4,128)}, s32[4,64]{1,0:T(4,128)S(1)}, /*index=5*/f32[4,6...) while((s32[]{:T(128)}, f32[4,32,64]{2,1,0:T(8,128)S(1)}, ...), condition=%wide.region_2.3_spmd.clone, body=%wide.region_0.2_spmd.clone.sunk | while | flops 28397956 | bytes 10237110 | solution.py:74
  124.3 5.8 copy.262
  133.6 4.5 dynamic_update_slice.11
  146.5 5.8 copy.262
  155.8 4.5 dynamic_update_slice.11
  168.7 5.8 copy.262
  190.9 5.8 copy.262
  208.7 12.7 %all-gather.3 = bf16[4,4,32]{2,1,0:T(4,128)(2,1)S(1)} all-gather(bf16[1,4,32]{2,1,0:T(4,128)(2,1)S(1)} %fusion.57), channel_id=4, replica_groups=mesh['grp'=2,'sp'=4,'tp'=4] {'sp'}, dimensions={0}, use_global_device_ids=true | all-gather | bytes 1280 | tf_op jit(solution)/shard_map/all_gather | solution.py:18
  221.4 13.4 %all-gather.1 = bf16[16,32,64]{2,1,0:T(8,128)(2,1)S(1)} all-gather(bf16[4,32,64]{2,1,0:T(8,128)(2,1)S(1)} %convert_element_type.257), channel_id=3, replica_groups=mesh['grp'=2,'sp'=4,'tp'=4] {'sp'}, dimensions={0}, use_global_device_ids=true | all-gather | bytes 81920 | tf_op jit(solution)/shard_map/all_gather | solution.py:18
  238.4 8.5 %all-reduce.6 = (bf16[4]{0:T(256)(128)(2,1)S(1)}, bf16[4]{0:T(256)(128)(2,1)S(1)}, bf16[4]{0:T(256)(128)(2,1)S(1)}, bf16[4]{0:T(256)(128)(2,1)S(1)}) all-reduce(bf16[4]{0:T(256)(128)(2,1)S(1)} %dynamic-update-slice.2, bf16[4]{0:T(256)(128)(2,1)S(1)} %dynamic-update-slice.3, ...), channel_id=1, replica_groups=mesh['grp'=2,'sp'=4,'tp'=4] {'sp'}, use_global_device_ids=true, to_apply=%add.2 | all-reduce | flops 16 | bytes 64
  246.9 15.9 %while.67 = (s32[]{:T(128)}, f32[4,32,64]{2,1,0:T(8,128)S(1)}, f32[]{:T(128)}, s32[]{:T(128)}, bf16[4,4,32,64]{3,2,1,0:T(8,128)(2,1)S(1)}, /*index=5*/bf16[4]{0:...) while((s32[]{:T(128)}, f32[4,32,64]{2,1,0:T(8,128)S(1)}, ...), condition=%wide.region_13.14_spmd.clone, body=%wide.region_12.13_spmd.clone.sunk | while | flops 41233 | bytes 83500 | solution.py:34
  269.5 9.6 %all_gather.60 = bf16[4,4,32]{2,1,0:T(4,128)(2,1)S(1)} all-gather(bf16[1,4,32]{2,1,0:T(4,128)(2,1)S(1)} %convert_element_type.252), channel_id=1, replica_groups=mesh['grp'=2,'sp'=4,'tp'=4] {'sp'}, dimensions={0}, use_global_device_ids=true | all-gather | bytes 1280 | tf_op jit(solution)/shard_map/all_gather | solution.py:18
  279.1 13.4 %all-gather = bf16[16,32,64]{2,1,0:T(8,128)(2,1)S(1)} all-gather(bf16[4,32,64]{2,1,0:T(8,128)(2,1)S(1)} %convert_element_type.247), channel_id=2, replica_groups=mesh['grp'=2,'sp'=4,'tp'=4] {'sp'}, dimensions={0}, use_global_device_ids=true | all-gather | bytes 81920 | tf_op jit(solution)/shard_map/all_gather | solution.py:18
  292.5 15.8 %while.65 = (s32[]{:T(128)}, f32[4,32,64]{2,1,0:T(8,128)S(1)}, f32[]{:T(128)}, s32[]{:T(128)}, bf16[4,4,32,64]{3,2,1,0:T(8,128)(2,1)S(1)}, /*index=5*/bf16[4]{0:...) while((s32[]{:T(128)}, f32[4,32,64]{2,1,0:T(8,128)S(1)}, ...), condition=%wide.region_5.6_spmd.clone, body=%wide.region_4.5_spmd.clone.sunk | while | flops 41229 | bytes 83438 | solution.py:34
  313.6 23.0 %reduce-scatter.3.cloned.1.call-done = bf16[256,512]{1,0:T(8,128)(2,1)} async-done(((bf16[256,2048]{1,0:T(8,128)(2,1)}), bf16[256,512]{1,0:T(8,128)(2,1)}) %reduce-scatter.3.cloned.1.call-update) | async-done | bytes 262160 | tf_op jit(solution)/shard_map/reduce_scatter | solution.py:161
  337.8 5.8 all-reduce.5
  347.4 15.5 %all-gather.9.cloned.1.call-done = bf16[256,2048]{1,0:T(8,128)(2,1)} async-done(((bf16[256,512]{1,0:T(8,128)(2,1)}), bf16[256,2048]{1,0:T(8,128)(2,1)}) %all-gather.9.cloned.1.call-update) | async-done | bytes 1048592 | tf_op jit(solution)/shard_map/all_gather | solution.py:174
  362.9 65.1 %all-gather.11.cloned.1.call-done = bf16[2048,768]{1,0:T(8,128)(2,1)} async-done(((bf16[512,768]{1,0:T(8,128)(2,1)}), bf16[2048,768]{1,0:T(8,128)(2,1)}) %all-gather.11.cloned.1.call-update) | async-done | bytes 3145744 | tf_op jit(solution)/shard_map/all_gather | solution.py:153
  432.1 59.5 %all-gather.13.cloned.1.call-done = bf16[2048,768]{1,0:T(8,128)(2,1)} async-done(((bf16[512,768]{1,0:T(8,128)(2,1)}), bf16[2048,768]{1,0:T(8,128)(2,1)}) %all-gather.13.cloned.1.call-update) | async-done | bytes 3145744 | tf_op jit(solution)/shard_map/all_gather | solution.py:154
  491.5 63.5 %all-gather.15.cloned.1.call-done = bf16[768,2048]{1,0:T(8,128)(2,1)} async-done(((bf16[768,512]{1,0:T(8,128)(2,1)}), bf16[768,2048]{1,0:T(8,128)(2,1)}) %all-gather.15.cloned.1.call-update) | async-done | bytes 3145744 | tf_op jit(solution)/shard_map/all_gather | solution.py:155
  555.1 6.2 %convolution_convert_fusion.1 = bf16[256,2048]{1,0:T(8,128)(2,1)} fusion(bf16[768,2048]{1,0:T(8,128)(2,1)} %all-gather.15.cloned.1.call-done, bf16[256,2048]{1,0:T(8,128)(2,1)S(1)} %copy-done.14, bf16[2048,768]{1,0:T(8,128)(2,1)} %all-gather.13.cloned.1.call-done, f32[256,768]{1,0:T(8,128)} %fusion.68), kind=kOutput, calls=%fused_computation.68 | convolution fusion | flops 1612316672 | bytes 9175040 | tf_op jit(solution)/shard_map/dot_general | solution.py:179
  561.3 23.6 %reduce-scatter.5.cloned.1.call-done = bf16[256,512]{1,0:T(8,128)(2,1)} async-done(((bf16[256,2048]{1,0:T(8,128)(2,1)}), bf16[256,512]{1,0:T(8,128)(2,1)}) %reduce-scatter.5.cloned.1.call-update) | async-done | bytes 262160 | tf_op jit(solution)/shard_map/reduce_scatter | solution.py:178
  586.2 5.8 all-reduce.4
  (321 shorter events, 151.8 us)
Async XLA Ops:
  6.5 305.4 %copy-start = (bf16[256,2048]{1,0:T(8,128)(2,1)S(1)}, bf16[256,2048]{1,0:T(8,128)(2,1)}, u32[]{:S(2)}) copy-start(bf16[256,2048]{1,0:T(8,128)(2,1)} %param.29) | copy-start | bytes 3145732
  6.5 330.2 %reduce-scatter.3.cloned.1.call-start = ((), (), s32[]{:S(2)}) async-start(), calls=%async_computation.2 | async-start | bytes 1310720 | tf_op jit(solution)/shard_map/reduce_scatter | solution.py:161
  14.6 98.4 %copy-start.5 = (f32[256,4,32]{0,2,1:T(8,128)}, f32[256,4,32]{0,2,1:T(8,128)S(1)}, u32[]{:S(2)}) copy-start(f32[256,4,32]{0,2,1:T(8,128)S(1)} %rev.19) | copy-start | bytes 393220
  16.6 3.8 copy-start.9
  17.4 3.0 copy-start.8
  114.7 2.9 copy-start.6
  117.5 117.2 %copy-start.17 = (u32[32]{0:T(128)S(1)}, u32[32]{0:T(128)}, u32[]{:S(2)}) copy-start(u32[32]{0:T(128)} %constant.182) | copy-start | bytes 388
  117.5 145.3 %copy-start.3 = (f32[4,64,4,64]{1,0,3,2:T(4,128)S(1)}, f32[4,64,4,64]{1,0,3,2:T(4,128)}, u32[]{:S(2)}) copy-start(f32[4,64,4,64]{1,0,3,2:T(4,128)} %get-tuple-element.457) | copy-start | bytes 786436
  206.3 102.0 %copy-start.11 = (s32[256]{0:T(256)S(1)}, s32[256]{0:T(256)}, u32[]{:S(2)}) copy-start(s32[256]{0:T(256)} %param.27) | copy-start | bytes 3076
  206.3 102.0 %copy-start.4 = (f32[4,64,4,64]{1,0,3,2:T(4,128)S(1)}, f32[4,64,4,64]{1,0,3,2:T(4,128)}, u32[]{:S(2)}) copy-start(f32[4,64,4,64]{1,0,3,2:T(4,128)} %get-tuple-element.452) | copy-start | bytes 786436
  206.3 102.4 %copy-start.7 = (f32[1,256,128]{1,2,0:T(8,128)S(1)}, f32[1,256,128]{1,2,0:T(8,128)}, u32[]{:S(2)}) copy-start(f32[1,256,128]{1,2,0:T(8,128)} %copy-done.6) | copy-start | bytes 393220
  206.3 104.9 %copy-start.10 = (bf16[256,128]{0,1:T(8,128)(2,1)S(1)}, bf16[256,128]{0,1:T(8,128)(2,1)}, u32[]{:S(2)}) copy-start(bf16[256,128]{0,1:T(8,128)(2,1)} %copy-done.9) | copy-start | bytes 196612
  246.9 65.1 %copy-start.15 = (bf16[256,256]{1,0:T(8,128)(2,1)S(1)}, bf16[256,256]{1,0:T(8,128)(2,1)}, u32[]{:S(2)}) copy-start(bf16[256,256]{1,0:T(8,128)(2,1)} %param.25) | copy-start | bytes 393220
  246.9 65.1 %copy-start.16 = (f32[256]{0:T(256)S(1)}, f32[256]{0:T(256)}, u32[]{:S(2)}) copy-start(f32[256]{0:T(256)} %param.28) | copy-start | bytes 3076
  292.5 21.1 %copy-start.12 = (f32[2,2048]{1,0:T(2,128)S(1)}, f32[2,2048]{1,0:T(2,128)}, u32[]{:S(2)}) copy-start(f32[2,2048]{1,0:T(2,128)} %param.31) | copy-start | bytes 49156
  292.5 21.1 %copy-start.13 = (f32[2,2048]{1,0:T(2,128)S(1)}, f32[2,2048]{1,0:T(2,128)}, u32[]{:S(2)}) copy-start(f32[2,2048]{1,0:T(2,128)} %param.32) | copy-start | bytes 49156
  292.5 44.2 %copy-start.1 = (bf16[256,512]{1,0:T(8,128)(2,1)S(1)}, bf16[256,512]{1,0:T(8,128)(2,1)}, u32[]{:S(2)}) copy-start(bf16[256,512]{1,0:T(8,128)(2,1)} %param.30) | copy-start | bytes 786436
  313.5 49.4 %all-gather.9.cloned.1.call-start = ((), (), s32[]{:S(2)}) async-start(), calls=%async_computation.3 | async-start | bytes 1310720 | tf_op jit(solution)/shard_map/all_gather | solution.py:174
  345.5 82.5 %all-gather.11.cloned.1.call-start = ((), (), s32[]{:S(2)}) async-start(), calls=%async_computation.4 | async-start | bytes 3932160 | tf_op jit(solution)/shard_map/all_gather | solution.py:153
  346.2 145.3 %all-gather.13.cloned.1.call-start = ((), (), s32[]{:S(2)}) async-start(), calls=%async_computation.5 | async-start | bytes 3932160 | tf_op jit(solution)/shard_map/all_gather | solution.py:154
  346.8 208.3 %all-gather.15.cloned.1.call-start = ((), (), s32[]{:S(2)}) async-start(), calls=%async_computation.6 | async-start | bytes 3932160 | tf_op jit(solution)/shard_map/all_gather | solution.py:155
  347.4 237.5 %reduce-scatter.5.cloned.1.call-start = ((), (), s32[]{:S(2)}) async-start(), calls=%async_computation.7 | async-start | bytes 1310720 | tf_op jit(solution)/shard_map/reduce_scatter | solution.py:178
  362.9 192.1 %copy-start.14 = (bf16[256,2048]{1,0:T(8,128)(2,1)S(1)}, bf16[256,2048]{1,0:T(8,128)(2,1)}, u32[]{:S(2)}) copy-start(bf16[256,2048]{1,0:T(8,128)(2,1)} %all-gather.9.cloned.1.call-done) | copy-start | bytes 3145732
  432.1 152.8 %copy-start.2 = (bf16[256,512]{1,0:T(8,128)(2,1)S(1)}, bf16[256,512]{1,0:T(8,128)(2,1)}, u32[]{:S(2)}) copy-start(bf16[256,512]{1,0:T(8,128)(2,1)} %reduce-scatter.3.cloned.1.call-done) | copy-start | bytes 786436
Sparse Core Ops, SparseCore 0:
  313.6 23.0 reduce-scatter.2
  345.6 17.3 all-gather.8
  364.5 63.4 all-gather.10
  429.4 62.0 all-gather.12
  492.9 62.0 all-gather.14
  561.4 23.4 reduce-scatter.4
where the time goes:
time: 603 us; the launch traced here: 600 us
  waiting for transfers between devices  252 us (42%)
  local copies, waits for them, and re-layouts  132 us (22%)
  other arithmetic  75.6 us (13%)
  blocking collectives  69.1 us (11%)
  loops' own time  32.7 us (5%)
  matrix products  22 us (4%)
  between operations  16.4 us (3%)
    all_gather x1, waiting for transfers between devices, on_device(): lax.all_gather(gate_weight, 'sp', axis=0, tiled=True)  65.1 us
    all_gather x1, waiting for transfers between devices, on_device(): lax.all_gather(down_weight, 'sp', axis=1, tiled=True)  63.5 us
    all_gather x1, waiting for transfers between devices, on_device(): lax.all_gather(up_weight, 'sp', axis=0, tiled=True)  59.5 us
    all_gather x4, blocking collectives, entering(): lax.all_gather(part.astype(kind), axis)  49 us
    while x8, local copies, waits for them, and re-layouts  46.3 us
    dynamic_update_slice x8, local copies, waits for them, and re-layouts, run_blocks(): lax.scan(advance, start, tuple((blocked(array) for array in (query, key_p...  35.8 us
    while x8, other arithmetic  25.3 us
    reduce_scatter x1, waiting for transfers between devices, on_device(): lax.psum_scatter(jnp.dot(inner, down_full, preferred_element_type=jnp.flo...  23.6 us
  transfers between devices with their start and end apart: 6, of which 6 were waited for; matrix products, arithmetic and copies ran while one was open for 1% of the time, Pallas kernels for 0%

commit v1 on v0

v1 whole, which is shorter than its diff:
```python
import functools

import jax
import jax.numpy as jnp
from jax import lax
from jax.experimental import pallas as pl
from jax.experimental.pallas import tpu as pltpu
from jax.sharding import PartitionSpec as P

DK = 32
DV = 64
EPS = 1e-06
F32 = jnp.float32
BF16 = jnp.bfloat16
HIGH = lax.Precision.HIGHEST
MESH = pl.DeviceIdType.MESH
VMEM = pltpu.VMEM


def dot(a, b, dims=((1,), (0,)), precision=None):
    return lax.dot_general(a, b, (dims, ((), ())), precision=precision, preferred_element_type=F32)


def iota(shape, axis):
    return lax.broadcasted_iota(jnp.int32, shape, axis)


def attend_kernel(q_ref, k_ref, v_ref, decay_ref, doc_ref, docrow_ref, out_ref, qf_ref, qb_ref, state_ref, aux_ref, acc):
    length, width = q_ref.shape
    heads = width // DK
    q = q_ref[...].astype(F32) * DK**-0.5
    k = k_ref[...].astype(F32)
    v = v_ref[...]
    row = iota((length, width), 0)
    far = iota((length, length), 0) ^ iota((length, length), 1)
    lane_head = (iota((length, 2 * width), 1) % width) // DK
    zero = jnp.zeros((length, width), F32)

    def scores(left, right):
        left, right = left.astype(BF16), right.astype(BF16)
        lanes = lane_head[:, : left.shape[1]]
        stacked = jnp.concatenate([jnp.where(lanes == h, left, jnp.zeros_like(left)) for h in range(heads)], axis=0)
        return dot(stacked, right, ((1,), (1,)))

    acc[...] = 2.0 * scores(q, k)
    total_f, total_b = decay_ref[0], decay_ref[1]
    prefix_f, suffix_b = total_f, total_b
    suffix_f, prefix_b = zero, zero
    span = 1
    while span < length:
        upper = (row & span) != 0
        left = jnp.concatenate(
            [jnp.where(upper, q * jnp.exp(prefix_f), 0.0), jnp.where(upper, 0.0, q * jnp.exp(suffix_b))], axis=1
        )
        right = jnp.concatenate(
            [jnp.where(upper, 0.0, k * jnp.exp(suffix_f)), jnp.where(upper, k * jnp.exp(prefix_b), 0.0)], axis=1
        )
        product = scores(left, right)
        for h in range(heads):
            rows = slice(h * length, (h + 1) * length)
            acc[rows] = jnp.where(far >= span, product[rows], acc[rows])

        def other(x):
            return jnp.where(upper, pltpu.roll(x, span, 0), pltpu.roll(x, length - span, 0))

        beside_f, beside_b = other(total_f), other(total_b)
        prefix_f = prefix_f + jnp.where(upper, beside_f, 0.0)
        suffix_f = suffix_f + jnp.where(upper, 0.0, beside_f)
        suffix_b = suffix_b + jnp.where(upper, 0.0, beside_b)
        prefix_b = prefix_b + jnp.where(upper, beside_b, 0.0)
        total_f, total_b = total_f + beside_f, total_b + beside_b
        span *= 2

    doc = doc_ref[...]
    same = doc == docrow_ref[...]
    value_head = iota((length, v.shape[1]), 1) // DV
    result = jnp.zeros((length, v.shape[1]), F32)
    for h in range(heads):
        weights = jnp.where(same, acc[h * length : (h + 1) * length], 0.0).astype(BF16)
        result = jnp.where(value_head == h, dot(weights, v), result)
    out_ref[...] = result
    qf_ref[...] = q * jnp.exp(prefix_f)
    qb_ref[...] = q * jnp.exp(suffix_b)

    first, last = doc[:1], doc[length - 1 :]
    own = (iota((width, v.shape[1]), 0) // DK) == (iota((width, v.shape[1]), 1) // DV)
    for i, (reach, edge) in enumerate(((suffix_f, last), (prefix_b, first))):
        kept = jnp.where(doc == edge, k * jnp.exp(reach), 0.0).astype(BF16)
        state = jnp.where(own, dot(kept, v, ((0,), (0,))), 0.0)
        packed = state[:DK]
        for h in range(1, heads):
            packed = packed + state[h * DK : (h + 1) * DK]
        state_ref[i * DK : (i + 1) * DK] = packed.astype(BF16)
    edge_row = iota((8, width), 0)
    aux = jnp.where(edge_row == 0, jnp.exp(total_f[:8]), jnp.exp(total_b[:8]))
    aux = jnp.where(edge_row == 2, first, aux)
    aux_ref[...] = jnp.where(edge_row == 3, last, aux)


def layer_kernel(
    sizes,
    local_ref,
    qf_ref,
    qb_ref,
    state_ref,
    aux_ref,
    doc_ref,
    outgate_ref,
    headgain_ref,
    outweight_ref,
    residual_ref,
    gain_ref,
    bias_ref,
    gate_hbm,
    up_hbm,
    down_hbm,
    result_ref,
    gate_all,
    up_all,
    down_all,
    states,
    auxes,
    sendbuf,
    landed,
    sendbuf2,
    landed2,
    features,
    moments,
    moments_in,
    small_send,
    small_recv,
    z_send,
    z_recv,
    y_send,
    y_recv,
    tp_send,
    tp_recv,
    local_sem,
):
    n_grp, n_sp, n_tp = sizes
    g, s, t = lax.axis_index("grp"), lax.axis_index("sp"), lax.axis_index("tp")
    length = local_ref.shape[0]
    own_width = residual_ref.shape[1]
    full_width = own_width * n_tp

    def around(axis, me, n, d):
        return {axis: lax.rem(me + d, n)}

    barrier = pltpu.get_barrier_semaphore()
    for axis, me, n in (("grp", g, n_grp), ("sp", s, n_sp), ("tp", t, n_tp)):
        for d in range(1, n):
            pl.semaphore_signal(barrier, inc=1, device_id=around(axis, me, n, d), device_id_type=MESH)
    pl.semaphore_wait(barrier, n_grp + n_sp + n_tp - 3)

    sent = []

    def remote(src, dst, ssem, rsem, to):
        return pltpu.make_async_remote_copy(
            src_ref=src, dst_ref=dst, send_sem=ssem, recv_sem=rsem, device_id=to, device_id_type=MESH
        )

    small = []
    for d in range(1, n_sp):
        to = around("sp", s, n_sp, d)
        for j, (src, dst) in enumerate(((state_ref, states), (aux_ref, auxes))):
            copy = remote(src, dst.at[d - 1], small_send.at[j, d - 1], small_recv.at[j, d - 1], to)
            copy.start()
            small.append(copy)

    whole = ((gate_hbm, gate_all), (up_hbm, up_all), (down_hbm, down_all))

    def part(p, origin, which):
        src, dst = whole[p]
        rows = src.shape[0] // n_grp
        return dst.at[origin, pl.ds(pl.multiple_of(which * rows, rows), rows), :]

    def own_part(p):
        src, _ = whole[p]
        rows = src.shape[0] // n_grp
        return src.at[pl.ds(pl.multiple_of(g * rows, rows), rows), :]

    def along(p, way, k, origin):
        step = 1 if way == 0 else -1
        src = own_part(p) if k == 0 else part(p, origin, g)
        return remote(
            src, part(p, origin, g), z_send.at[p, way, k], z_recv.at[p, way, k], {"sp": lax.rem(s + step + n_sp, n_sp)}
        )

    def across(p, way, k, origin, d):
        return remote(
            part(p, origin, g), part(p, origin, g), y_send.at[p, way, k, d - 1], y_recv.at[p, way, k, d - 1],
            around("grp", g, n_grp, d),
        )

    def inside(x):
        return (x >= 0) & (x < n_sp)

    for p in range(3):
        for way in range(2):
            step = 1 if way == 0 else -1

            @pl.when(inside(s + step))
            def _(p=p, way=way):
                along(p, way, 0, s).start()

    own_copies = []
    for p in range(3):
        copy = pltpu.make_async_copy(whole[p][0], whole[p][1].at[s], local_sem.at[p])
        copy.start()
        own_copies.append(copy)

    def relay(k, p):
        for way in range(2):
            step = 1 if way == 0 else -1
            origin = s - step * k

            @pl.when(inside(origin))
            def _(way=way, step=step, origin=origin):
                along(p, way, k - 1, origin).wait_recv()
                if k < n_sp - 1:

                    @pl.when(inside(s + step))
                    def _():
                        along(p, way, k, origin).start()

                for d in range(1, n_grp):
                    across(p, way, k, origin, d).start()

    def finish_across(k, p):
        for way in range(2):
            origin = s - (1 if way == 0 else -1) * k

            @pl.when(inside(origin))
            def _(way=way, origin=origin):
                for d in range(1, n_grp):
                    arrived = part(p, origin, lax.rem(g - d + n_grp, n_grp))
                    sems = (y_send.at[p, way, k, d - 1], y_recv.at[p, way, k, d - 1])
                    remote(arrived, arrived, *sems, around("grp", g, n_grp, d)).wait_recv()

    events = [(k, p) for k in range(1, n_sp) for p in range(3)]
    cursor = [0]

    def pump(count):
        for k, p in events[cursor[0] : cursor[0] + count]:
            relay(k, p)
        cursor[0] += count

    def to_tp(kind, src_of, dst_of):
        copies = []
        for d in range(1, n_tp):
            to = lax.rem(t + d, n_tp)
            copy = remote(
                src_of(to), dst_of(d), tp_send.at[kind, d - 1], tp_recv.at[kind, d - 1], {"tp": to}
            )
            copy.start()
            copies.append(copy)
        sent.extend(copies)
        return copies

    for copy in small:
        copy.wait_recv()
    sent.extend(small)
    doc = doc_ref[...]
    first, last = doc[:1], doc[length - 1 :]
    width = qf_ref.shape[1]
    heads = width // DK
    value_width = local_ref.shape[1]
    own = (iota((width, value_width), 0) // DK) == (iota((width, value_width), 1) // DV)
    attended = local_ref[...]
    for back in range(2):
        query = (qb_ref if back else qf_ref)[...]
        edge = last if back else first
        reach = jnp.ones((1, width), F32)
        entering = jnp.zeros((length, value_width), F32)
        for d in range(1, n_sp):
            slot = (n_sp - d if back else d) - 1
            valid = (s + d < n_sp) if back else (s - d >= 0)
            aux = auxes[slot]
            facing = aux[2:3] if back else aux[3:4]
            joined = jnp.where(facing == edge, jnp.where(valid, 1.0, 0.0), 0.0)
            state = states[slot, back * DK : (back + 1) * DK]
            state = jnp.where(own, jnp.concatenate([state] * heads, axis=0), jnp.zeros((), BF16))
            entering = entering + dot((query * jnp.where(joined > 0.0, reach, 0.0)).astype(BF16), state)
            reach = reach * aux[back : back + 1]
        attended = attended + jnp.where(doc == edge, entering, 0.0)
    group = (iota((value_width, value_width), 0) // DV) == (iota((value_width, value_width), 1) // DV)
    mean_square = dot(attended * attended, jnp.where(group, 1.0 / DV, 0.0), precision=HIGH)
    u = outgate_ref[...].astype(F32)
    mixed = attended * lax.rsqrt(mean_square + EPS) * headgain_ref[...] * (u / (1.0 + jnp.exp(-u)))
    mixed = mixed.astype(BF16)
    for i in range(n_tp):
        sendbuf[i] = dot(mixed, outweight_ref[:, i * own_width : (i + 1) * own_width]).astype(BF16)

    def norm(stream, kind):
        ones = jnp.ones((8, own_width), F32)
        sums = dot(ones, stream, ((1,), (1,)), HIGH)
        squares = dot(ones, stream * stream, ((1,), (1,)), HIGH)
        moments[kind] = jnp.where(iota((8, length), 0) == 0, sums, squares)
        copies = to_tp(2 + kind, lambda to: moments.at[kind], lambda d: moments_in.at[kind, d - 1])
        for copy in copies:
            copy.wait_recv()
        total = moments[kind]
        for d in range(1, n_tp):
            total = total + moments_in[kind, d - 1]
        eye = jnp.where(iota((length, length), 0) == iota((length, length), 1), 1.0, 0.0)
        total = dot(eye, total, ((1,), (1,)), HIGH) / full_width
        middle = total[:, 0:1]
        spread = total[:, 1:2] - middle * middle
        return (stream - middle) * lax.rsqrt(spread + EPS) * gain_ref[kind, t] + bias_ref[kind, t]

    copies = to_tp(0, lambda to: sendbuf.at[to], lambda d: landed.at[d - 1])
    pump(1)
    for copy in copies:
        copy.wait_recv()
    stream = sendbuf[t].astype(F32)
    for d in range(1, n_tp):
        stream = stream + landed[d - 1].astype(F32)
    settled = norm(residual_ref[...].astype(F32) + stream, 0)
    features[t] = settled.astype(BF16)
    copies = to_tp(1, lambda to: features.at[t], lambda d: features.at[t])
    pump(2)
    for copy in copies:
        copy.wait_recv()

    pump(len(events) - cursor[0] - 1)
    own_copies[0].wait()
    own_copies[1].wait()
    for k in range(1, n_sp):
        for p in range(2):
            finish_across(k, p)
    depth = gate_hbm.shape[0]

    def project(weights):
        out = None
        for i in range(n_tp):
            block = own_width // depth
            term = dot(features[i], weights[i * block : (i + 1) * block].reshape(own_width, weights.shape[2]))
            out = term if out is None else out + term
        return out

    gate = project(gate_all)
    inner = (gate / (1.0 + jnp.exp(-gate)) * project(up_all)).astype(BF16)

    pump(1)
    own_copies[2].wait()
    for k in range(1, n_sp):
        finish_across(k, 2)
    piece = down_hbm.shape[1]
    for i in range(n_sp):
        owner, at = (i * piece) // own_width, (i * piece) % own_width
        sendbuf2[owner, :, at : at + piece] = dot(inner, down_all[i]).astype(BF16)
    copies = to_tp(4, lambda to: sendbuf2.at[to], lambda d: landed2.at[d - 1])
    for copy in copies:
        copy.wait_recv()
    down = sendbuf2[t].astype(F32)
    for d in range(1, n_tp):
        down = down + landed2[d - 1].astype(F32)
    result_ref[...] = norm(settled + 0.5 * down, 1).astype(BF16)

    for copy in sent:
        copy.wait_send()
    for p in range(3):
        for way in range(2):
            step = 1 if way == 0 else -1
            for k in range(n_sp - 1):

                @pl.when(inside(s + step) & inside(s - step * k))
                def _(p=p, way=way, k=k, step=step):
                    along(p, way, k, s - step * k).wait_send()

            for k in range(1, n_sp):

                @pl.when(inside(s - step * k))
                def _(p=p, way=way, k=k, step=step):
                    for d in range(1, n_grp):
                        across(p, way, k, s - step * k, d).wait_send()


def on_device(
    sizes,
    queries,
    key_rows,
    value_rows,
    out_gate,
    log_decay,
    doc_ids,
    head_gain,
    out_weight,
    residual,
    norm_gain,
    norm_bias,
    gate_weight,
    up_weight,
    down_weight,
):
    n_grp, n_sp, n_tp = sizes
    length, width = queries.shape
    value_width = value_rows.shape[1]
    own_width = residual.shape[1]
    heads = width // DK
    doc = doc_ids.astype(F32)
    doc_column, doc_row = doc[:, None], doc[None, :]
    local, qf, qb, state, aux = pl.pallas_call(
        attend_kernel,
        out_shape=(
            jax.ShapeDtypeStruct((length, value_width), F32),
            jax.ShapeDtypeStruct((length, width), F32),
            jax.ShapeDtypeStruct((length, width), F32),
            jax.ShapeDtypeStruct((2 * DK, value_width), BF16),
            jax.ShapeDtypeStruct((8, width), F32),
        ),
        scratch_shapes=[VMEM((heads * length, length), F32)],
        compiler_params=pltpu.CompilerParams(vmem_limit_bytes=24 * 2**20),
        name="attend",
    )(queries, key_rows, value_rows, log_decay, doc_column, doc_row)

    vm = pl.BlockSpec(memory_space=VMEM)
    hbm = pl.BlockSpec(memory_space=pl.ANY)
    dma = pltpu.SemaphoreType.DMA
    hops = max(n_grp - 1, 1)
    return pl.pallas_call(
        functools.partial(layer_kernel, sizes),
        out_shape=jax.ShapeDtypeStruct((length, own_width), BF16),
        in_specs=[vm] * 12 + [hbm] * 3,
        out_specs=vm,
        scratch_shapes=[
            VMEM((n_sp,) + gate_weight.shape, BF16),
            VMEM((n_sp,) + up_weight.shape, BF16),
            VMEM((n_sp,) + down_weight.shape, BF16),
            VMEM((n_sp - 1, 2 * DK, value_width), BF16),
            VMEM((n_sp - 1, 8, width), F32),
            VMEM((n_tp, length, own_width), BF16),
            VMEM((n_tp - 1, length, own_width), BF16),
            VMEM((n_tp, length, own_width), BF16),
            VMEM((n_tp - 1, length, own_width), BF16),
            VMEM((n_tp, length, own_width), BF16),
            VMEM((2, 8, length), F32),
            VMEM((2, n_tp - 1, 8, length), F32),
            dma((2, n_sp - 1)),
            dma((2, n_sp - 1)),
            dma((3, 2, n_sp)),
            dma((3, 2, n_sp)),
            dma((3, 2, n_sp, hops)),
            dma((3, 2, n_sp, hops)),
            dma((5, n_tp - 1)),
            dma((5, n_tp - 1)),
            dma((3,)),
        ],
        compiler_params=pltpu.CompilerParams(
            collective_id=0, has_side_effects=True, vmem_limit_bytes=48 * 2**20
        ),
        name="layer",
    )(
        local,
        qf,
        qb,
        state,
        aux,
        doc_column,
        out_gate,
        head_gain[None, :],
        out_weight,
        residual,
        norm_gain.reshape(2, n_tp, 1, own_width),
        norm_bias.reshape(2, n_tp, 1, own_width),
        gate_weight,
        up_weight,
        down_weight,
    )


def solution(mesh):
    sizes = tuple(mesh.shape[axis] for axis in ("grp", "sp", "tp"))
    in_specs = (
        P(("grp", "sp"), "tp"),
        P(("grp", "sp"), "tp"),
        P(("grp", "sp"), "tp"),
        P(("grp", "sp"), "tp"),
        P(None, ("grp", "sp"), "tp"),
        P(("grp", "sp")),
        P("tp"),
        P("tp", None),
        P(("grp", "sp"), "tp"),
        P(),
        P(),
        P("sp", "tp"),
        P("sp", "tp"),
        P("tp", "sp"),
    )
    return jax.shard_map(
        functools.partial(on_device, sizes),
        mesh=mesh,
        in_specs=in_specs,
        out_specs=P(("grp", "sp"), "tp"),
        check_vma=False,
    )
```

time: 603 us -> 132 us (0.22)
  waiting for transfers between devices: 252 us -> 0 us
  local copies, waits for them, and re-layouts: 132 us -> 11.9 us
  Pallas kernels: 0 us -> 119 us
  other arithmetic: 75.6 us -> 0.75 us
  blocking collectives: 69.1 us -> 0 us
  loops' own time: 32.7 us -> 0 us
  matrix products: 22 us -> 0 us
  between operations: 16.4 us -> 0.06 us
    all_gather x4 -> x0, waiting for transfers between devices: 204 us -> none  [the longest x1 65.1 us: on_device(): lax.all_gather(gate_weight, 'sp', axis=0, tiled=True)]
    pallas_call x0 -> x2, Pallas kernels: none -> 119 us  [the longest x1 117 us: on_device(): pl.pallas_call(functools.partial(layer_kernel, sizes), out_shape=jax.Shap...]
    all_gather x4 -> x0, blocking collectives: 49 us -> none  [entering(): lax.all_gather(part.astype(kind), axis)]
    reduce_scatter x2 -> x0, waiting for transfers between devices: 46.6 us -> none  [the longest x1 23.6 us: on_device(): lax.psum_scatter(jnp.dot(inner, down_full, preferred_element_type=jnp.flo...]
    while x8 -> x0, local copies, waits for them, and re-layouts: 46.3 us -> none
    dynamic_update_slice x8 -> x0, local copies, waits for them, and re-layouts: 35.8 us -> none  [run_blocks(): lax.scan(advance, start, tuple((blocked(array) for array in (query, key_p...]
    another operation x4 -> x0, loops' own time: 32.7 us -> none  [the longest x2 21.2 us: entering(): return lax.fori_loop(0, peers, hop, start)]
    while x8 -> x0, other arithmetic: 25.3 us -> none
  transfers between devices with their start and end apart: 6 -> 0, of which waited for: 6 -> 0; matrix products, arithmetic and copies ran while one was open for 1% -> 0% of each run, Pallas kernels for 0% -> 0%
where the time goes in v1:
time: 132 us
  Pallas kernels  119 us (90%)
  local copies, waits for them, and re-layouts  11.9 us (9%)
    pallas_call x1, Pallas kernels, on_device(): pl.pallas_call(functools.partial(layer_kernel, sizes), out_shape=jax.Shap...  117 us
    unnamed x23, local copies, waits for them, and re-layouts  10.2 us

profile of v1, /device:TPU:0, one launch (start us, length us, event | category | flops | bytes accessed | tf_op | source)
XLA Modules:
  0.0 131.8 jit_solution(13600520587974219056)
XLA Ops:
  0.0 0.0 copy-start.1
  0.0 0.8 convert_element_type.3
  0.8 0.7 reshape.6.gain_ref
  1.5 0.7 reshape.7.bias_ref
  2.3 0.1 copy.15.doc_ref
  2.4 0.0 copy-start.4
  2.4 0.9 copy-done.4
  3.4 0.0 copy-start.6
  3.4 0.9 copy-done.6
  4.3 0.0 copy-start.8
  4.3 0.8 copy-done.8
  5.1 0.0 copy-start.9
  5.1 0.8 copy-done.9
  5.9 1.9 %attend.1 = (f32[256,256]{1,0:T(8,128)S(1)}, f32[256,128]{1,0:T(8,128)S(1)}, f32[256,128]{1,0:T(8,128)S(1)}, bf16[64,256]{1,0:T(8,128)(2,1)S(1)}, f32[8,128]{1,0:T(8,128)S(1)}) custom-call(bf16[256,128]{1,0:T(8,128)(2,1)S(1)} %copy-done.8, bf16[256,128]{1,0:T(8,128)(2,1)S(1)} %copy-done.9, bf16[256,256]{1,0:T(8,128)(2,1)S(1)} %copy-done.6, ...), custom_call_target="tpu_custom_call" | custom-call | tf_op jit(solution)/shard_map/attend/pallas_call | solution.py:403
  7.8 0.0 copy-start.10
  7.9 0.0 copy-done.1
  7.9 0.7 copy-done.10
  8.5 0.0 copy-start
  8.5 1.2 copy-done
  9.8 0.0 copy-start.2
  9.8 1.1 copy-done.2
  10.9 0.0 copy-start.3
  10.9 1.1 copy-done.3
  12.0 0.0 copy-start.5
  12.0 0.9 copy-done.5
  13.0 0.0 copy-start.7
  13.0 0.9 copy-done.7
  13.9 117.2 %layer.1 = bf16[256,512]{1,0:T(8,128)(2,1)S(1)} custom-call(f32[256,256]{1,0:T(8,128)S(1)} %get-tuple-element.10.local_ref, f32[256,128]{1,0:T(8,128)S(1)} %get-tuple-element.11.qf_ref, f32[256,128]{1,0:T(8,128)S(1)} %get-tuple-element.12.qb_ref, bf16[64,256]{1,0:T(8,128)(2,1)S(1)} %get-tuple-element.13.state_ref, f32[8,128]{1,0:T(8,128)S(1)} %get-tuple-element.14.aux_ref, ...), custom_call_target="tpu_custom_call" | custom-call | tf_op jit(solution)/shard_map/layer/pallas_call | solution.py:421
  131.0 0.7 copy.18
Async XLA Ops:
  0.0 7.9 %copy-start.1 = (bf16[512,768]{1,0:T(8,128)(2,1)S(1)}, bf16[512,768]{1,0:T(8,128)(2,1)}, u32[]{:S(2)}) copy-start(bf16[512,768]{1,0:T(8,128)(2,1)} %gate_hbm.1) | copy-start | bytes 2359300
  2.4 1.0 copy-start.4
  3.4 0.9 copy-start.6
  4.3 0.8 copy-start.8
  5.1 0.8 copy-start.9
  7.8 0.7 copy-start.10
  8.5 1.2 copy-start
  9.8 1.1 copy-start.2
  10.9 1.1 copy-start.3
  12.0 0.9 copy-start.5
  13.0 0.9 copy-start.7

commit v2 on v1

--- a/solution.py
+++ b/solution.py
@@ -15,6 +15,7 @@
 HIGH = lax.Precision.HIGHEST
 MESH = pl.DeviceIdType.MESH
 VMEM = pltpu.VMEM
+PIECES = ((0, 0, 2), (0, 1, 2), (1, 0, 1), (2, 0, 2), (2, 1, 2))
 
 
 def dot(a, b, dims=((1,), (0,)), precision=None):
@@ -25,7 +26,7 @@
     return lax.broadcasted_iota(jnp.int32, shape, axis)
 
 
-def attend_kernel(q_ref, k_ref, v_ref, decay_ref, doc_ref, docrow_ref, out_ref, qf_ref, qb_ref, state_ref, aux_ref, acc):
+def attend(q_ref, k_ref, v_ref, decay_ref, doc, doc_row, out_ref, qf_ref, qb_ref, state_ref, aux_ref, acc):
     length, width = q_ref.shape
     heads = width // DK
     q = q_ref[...].astype(F32) * DK**-0.5
@@ -71,8 +72,7 @@
         total_f, total_b = total_f + beside_f, total_b + beside_b
         span *= 2
 
-    doc = doc_ref[...]
-    same = doc == docrow_ref[...]
+    same = doc == doc_row
     value_head = iota((length, v.shape[1]), 1) // DV
     result = jnp.zeros((length, v.shape[1]), F32)
     for h in range(heads):
@@ -97,54 +97,43 @@
     aux_ref[...] = jnp.where(edge_row == 3, last, aux)
 
 
-def layer_kernel(
-    sizes,
-    local_ref,
-    qf_ref,
-    qb_ref,
-    state_ref,
-    aux_ref,
-    doc_ref,
-    outgate_ref,
-    headgain_ref,
-    outweight_ref,
-    residual_ref,
-    gain_ref,
-    bias_ref,
-    gate_hbm,
-    up_hbm,
-    down_hbm,
-    result_ref,
-    gate_all,
-    up_all,
-    down_all,
-    states,
-    auxes,
-    sendbuf,
-    landed,
-    sendbuf2,
-    landed2,
-    features,
-    moments,
-    moments_in,
-    small_send,
-    small_recv,
-    z_send,
-    z_recv,
-    y_send,
-    y_recv,
-    tp_send,
-    tp_recv,
-    local_sem,
-):
+def layer_kernel(sizes, *refs):
+    (
+        q_hbm, k_hbm, v_hbm, outgate_hbm, decay_hbm, docrow_hbm, headgain_hbm, outweight_hbm, residual_hbm,
+        gain_hbm, bias_hbm, gate_hbm, up_hbm, down_hbm, result_ref,
+        q_ref, k_ref, v_ref, outgate_ref, decay_ref, docrow_ref, headgain_ref, outweight_ref, residual_ref,
+        gain_ref, bias_ref, local_ref, qf_ref, qb_ref, state_ref, aux_ref, acc, inner_ref,
+        gate_all, up_all, down_all, states, auxes, sendbuf, landed, sendbuf2, landed2, features, moments,
+        moments_in, small_send, small_recv, z_send, z_recv, y_send, y_recv, tp_send, tp_recv, local_sem, in_sem,
+    ) = refs
     n_grp, n_sp, n_tp = sizes
     g, s, t = lax.axis_index("grp"), lax.axis_index("sp"), lax.axis_index("tp")
-    length = local_ref.shape[0]
-    own_width = residual_ref.shape[1]
+    length = q_hbm.shape[0]
+    own_width = residual_hbm.shape[1]
     full_width = own_width * n_tp
 
     def around(axis, me, n, d):
         return {axis: lax.rem(me + d, n)}
+
+    mine = pl.ds(pl.multiple_of(t * own_width, own_width), own_width)
+    loads = []
+    for i, (src, dst) in enumerate(
+        (
+            (decay_hbm, decay_ref),
+            (q_hbm, q_ref),
+            (k_hbm, k_ref),
+            (docrow_hbm, docrow_ref),
+            (v_hbm, v_ref),
+            (outgate_hbm, outgate_ref),
+            (headgain_hbm, headgain_ref),
+            (outweight_hbm, outweight_ref),
+            (residual_hbm, residual_ref),
+            (gain_hbm.at[:, mine], gain_ref),
+            (bias_hbm.at[:, mine], bias_ref),
+        )
+    ):
+        loads.append(pltpu.make_async_copy(src, dst, in_sem.at[i]))
+        loads[-1].start()
 
     barrier = pltpu.get_barrier_semaphore()
     for axis, me, n in (("grp", g, n_grp), ("sp", s, n_sp), ("tp", t, n_tp)):
@@ -159,25 +148,23 @@
             src_ref=src, dst_ref=dst, send_sem=ssem, recv_sem=rsem, device_id=to, device_id_type=MESH
         )
 
-    small = []
-    for d in range(1, n_sp):
-        to = around("sp", s, n_sp, d)
-        for j, (src, dst) in enumerate(((state_ref, states), (aux_ref, auxes))):
-            copy = remote(src, dst.at[d - 1], small_send.at[j, d - 1], small_recv.at[j, d - 1], to)
-            copy.start()
-            small.append(copy)
-
     whole = ((gate_hbm, gate_all), (up_hbm, up_all), (down_hbm, down_all))
+    pieces = PIECES
+    n_up = sum(1 for which, _, _ in pieces if which < 2)
+
+    def rows_of(p, which):
+        weight, share, shares = pieces[p]
+        src, dst = whole[weight]
+        rows = src.shape[0] // (n_grp * shares)
+        return src, dst, pl.ds(pl.multiple_of((which * shares + share) * rows, rows), rows)
 
     def part(p, origin, which):
-        src, dst = whole[p]
-        rows = src.shape[0] // n_grp
-        return dst.at[origin, pl.ds(pl.multiple_of(which * rows, rows), rows), :]
+        _, dst, rows = rows_of(p, which)
+        return dst.at[origin, rows, :]
 
     def own_part(p):
-        src, _ = whole[p]
-        rows = src.shape[0] // n_grp
-        return src.at[pl.ds(pl.multiple_of(g * rows, rows), rows), :]
+        src, _, rows = rows_of(p, g)
+        return src.at[rows, :]
 
     def along(p, way, k, origin):
         step = 1 if way == 0 else -1
@@ -195,19 +182,17 @@
     def inside(x):
         return (x >= 0) & (x < n_sp)
 
-    for p in range(3):
+    def start_own(p):
         for way in range(2):
             step = 1 if way == 0 else -1
 
             @pl.when(inside(s + step))
-            def _(p=p, way=way):
+            def _(way=way):
                 along(p, way, 0, s).start()
 
     own_copies = []
     for p in range(3):
-        copy = pltpu.make_async_copy(whole[p][0], whole[p][1].at[s], local_sem.at[p])
-        copy.start()
-        own_copies.append(copy)
+        own_copies.append(pltpu.make_async_copy(whole[p][0], whole[p][1].at[s], local_sem.at[p]))
 
     def relay(k, p):
         for way in range(2):
@@ -237,7 +222,7 @@
                     sems = (y_send.at[p, way, k, d - 1], y_recv.at[p, way, k, d - 1])
                     remote(arrived, arrived, *sems, around("grp", g, n_grp, d)).wait_recv()
 
-    events = [(k, p) for k in range(1, n_sp) for p in range(3)]
+    events = [(k, p) for k in range(1, n_sp) for p in range(len(pieces))]
     cursor = [0]
 
     def pump(count):
@@ -257,10 +242,34 @@
         sent.extend(copies)
         return copies
 
+    start_own(0)
+    for load in loads[:5]:
+        load.wait()
+    doc_row = docrow_ref[...]
+    eye = iota((length, length), 0) == iota((length, length), 1)
+    doc = jnp.sum(jnp.where(eye, doc_row, 0), axis=1, keepdims=True).astype(F32)
+    attend(
+        q_ref, k_ref, v_ref, decay_ref, doc, doc_row.astype(F32), local_ref, qf_ref, qb_ref, state_ref, aux_ref, acc
+    )
+    small = []
+    for d in range(1, n_sp):
+        to = around("sp", s, n_sp, d)
+        for j, (src, dst) in enumerate(((state_ref, states), (aux_ref, auxes))):
+            copy = remote(src, dst.at[d - 1], small_send.at[j, d - 1], small_recv.at[j, d - 1], to)
+            copy.start()
+            small.append(copy)
+
+    for p in range(1, len(pieces)):
+        start_own(p)
+    for copy in own_copies:
+        copy.start()
+    for load in loads[5:]:
+        load.wait()
+    pump(1)
+
     for copy in small:
         copy.wait_recv()
     sent.extend(small)
-    doc = doc_ref[...]
     first, last = doc[:1], doc[length - 1 :]
     width = qf_ref.shape[1]
     heads = width // DK
@@ -302,16 +311,16 @@
         total = moments[kind]
         for d in range(1, n_tp):
             total = total + moments_in[kind, d - 1]
-        eye = jnp.where(iota((length, length), 0) == iota((length, length), 1), 1.0, 0.0)
-        total = dot(eye, total, ((1,), (1,)), HIGH) / full_width
+        total = dot(jnp.where(eye, 1.0, 0.0), total, ((1,), (1,)), HIGH) / full_width
         middle = total[:, 0:1]
         spread = total[:, 1:2] - middle * middle
-        return (stream - middle) * lax.rsqrt(spread + EPS) * gain_ref[kind, t] + bias_ref[kind, t]
+        return (stream - middle) * lax.rsqrt(spread + EPS) * gain_ref[kind : kind + 1] + bias_ref[kind : kind + 1]
 
     copies = to_tp(0, lambda to: sendbuf.at[to], lambda d: landed.at[d - 1])
-    pump(1)
+    pump(2)
     for copy in copies:
         copy.wait_recv()
+    pump(1)
     stream = sendbuf[t].astype(F32)
     for d in range(1, n_tp):
         stream = stream + landed[d - 1].astype(F32)
@@ -322,11 +331,11 @@
     for copy in copies:
         copy.wait_recv()
 
-    pump(len(events) - cursor[0] - 1)
-    own_copies[0].wait()
-    own_copies[1].wait()
+    pump(len(events) - cursor[0])
+    for copy in own_copies:
+        copy.wait()
     for k in range(1, n_sp):
-        for p in range(2):
+        for p in range(n_up):
             finish_across(k, p)
     depth = gate_hbm.shape[0]
 
@@ -339,17 +348,51 @@
         return out
 
     gate = project(gate_all)
-    inner = (gate / (1.0 + jnp.exp(-gate)) * project(up_all)).astype(BF16)
-
-    pump(1)
-    own_copies[2].wait()
-    for k in range(1, n_sp):
-        finish_across(k, 2)
+    inner_ref[...] = (gate / (1.0 + jnp.exp(-gate)) * project(up_all)).astype(BF16)
+
     piece = down_hbm.shape[1]
-    for i in range(n_sp):
-        owner, at = (i * piece) // own_width, (i * piece) % own_width
-        sendbuf2[owner, :, at : at + piece] = dot(inner, down_all[i]).astype(BF16)
-    copies = to_tp(4, lambda to: sendbuf2.at[to], lambda d: landed2.at[d - 1])
+    if piece == own_width:
+        def deliver(owner):
+            d = lax.rem(owner - t + n_tp, n_tp)
+            at = jnp.maximum(d - 1, 0)
+            return remote(
+                sendbuf2.at[owner], landed2.at[at], tp_send.at[4, at], tp_recv.at[4, at], {"tp": owner}
+            )
+
+        def one_block(origin):
+            sendbuf2[origin] = dot(inner_ref[...], down_all[origin]).astype(BF16)
+
+            @pl.when(origin != t)
+            def _():
+                deliver(origin).start()
+
+        one_block(s)
+        for k in range(1, n_sp):
+            for p in range(n_up, len(pieces)):
+                finish_across(k, p)
+            for way in range(2):
+                origin = s - (1 if way == 0 else -1) * k
+
+                @pl.when(inside(origin))
+                def _(origin=origin):
+                    one_block(origin)
+
+        copies = [
+            remote(
+                sendbuf2.at[lax.rem(t + d, n_tp)], landed2.at[d - 1], tp_send.at[4, d - 1], tp_recv.at[4, d - 1],
+                {"tp": lax.rem(t + d, n_tp)},
+            )
+            for d in range(1, n_tp)
+        ]
+        sent.extend(copies)
+    else:
+        for k in range(1, n_sp):
+            for p in range(n_up, len(pieces)):
+                finish_across(k, p)
+        for i in range(n_sp):
+            owner, at = (i * piece) // own_width, (i * piece) % own_width
+            sendbuf2[owner, :, at : at + piece] = dot(inner_ref[...], down_all[i]).astype(BF16)
+        copies = to_tp(4, lambda to: sendbuf2.at[to], lambda d: landed2.at[d - 1])
     for copy in copies:
         copy.wait_recv()
     down = sendbuf2[t].astype(F32)
@@ -359,7 +402,7 @@
 
     for copy in sent:
         copy.wait_send()
-    for p in range(3):
+    for p in range(len(pieces)):
         for way in range(2):
             step = 1 if way == 0 else -1
             for k in range(n_sp - 1):
@@ -398,22 +441,6 @@
     value_width = value_rows.shape[1]
     own_width = residual.shape[1]
     heads = width // DK
-    doc = doc_ids.astype(F32)
-    doc_column, doc_row = doc[:, None], doc[None, :]
-    local, qf, qb, state, aux = pl.pallas_call(
-        attend_kernel,
-        out_shape=(
-            jax.ShapeDtypeStruct((length, value_width), F32),
-            jax.ShapeDtypeStruct((length, width), F32),
-            jax.ShapeDtypeStruct((length, width), F32),
-            jax.ShapeDtypeStruct((2 * DK, value_width), BF16),
-            jax.ShapeDtypeStruct((8, width), F32),
-        ),
-        scratch_shapes=[VMEM((heads * length, length), F32)],
-        compiler_params=pltpu.CompilerParams(vmem_limit_bytes=24 * 2**20),
-        name="attend",
-    )(queries, key_rows, value_rows, log_decay, doc_column, doc_row)
-
     vm = pl.BlockSpec(memory_space=VMEM)
     hbm = pl.BlockSpec(memory_space=pl.ANY)
     dma = pltpu.SemaphoreType.DMA
@@ -421,9 +448,27 @@
     return pl.pallas_call(
         functools.partial(layer_kernel, sizes),
         out_shape=jax.ShapeDtypeStruct((length, own_width), BF16),
-        in_specs=[vm] * 12 + [hbm] * 3,
+        in_specs=[hbm] * 14,
         out_specs=vm,
         scratch_shapes=[
+            VMEM((length, width), BF16),
+            VMEM((length, width), BF16),
+            VMEM((length, value_width), BF16),
+            VMEM((length, value_width), BF16),
+            VMEM((2, length, width), F32),
+            VMEM((1, length), jnp.int32),
+            VMEM((1, value_width), F32),
+            VMEM(out_weight.shape, BF16),
+            VMEM((length, own_width), BF16),
+            VMEM((2, own_width), F32),
+            VMEM((2, own_width), F32),
+            VMEM((length, value_width), F32),
+            VMEM((length, width), F32),
+            VMEM((length, width), F32),
+            VMEM((2 * DK, value_width), BF16),
+            VMEM((8, width), F32),
+            VMEM((heads * length, length), F32),
+            VMEM((length, gate_weight.shape[1]), BF16),
             VMEM((n_sp,) + gate_weight.shape, BF16),
             VMEM((n_sp,) + up_weight.shape, BF16),
             VMEM((n_sp,) + down_weight.shape, BF16),
@@ -438,31 +483,31 @@
             VMEM((2, n_tp - 1, 8, length), F32),
             dma((2, n_sp - 1)),
             dma((2, n_sp - 1)),
-            dma((3, 2, n_sp)),
-            dma((3, 2, n_sp)),
-            dma((3, 2, n_sp, hops)),
-            dma((3, 2, n_sp, hops)),
+            dma((len(PIECES), 2, n_sp)),
+            dma((len(PIECES), 2, n_sp)),
+            dma((len(PIECES), 2, n_sp, hops)),
+            dma((len(PIECES), 2, n_sp, hops)),
             dma((5, n_tp - 1)),
             dma((5, n_tp - 1)),
             dma((3,)),
+            dma((11,)),
         ],
         compiler_params=pltpu.CompilerParams(
-            collective_id=0, has_side_effects=True, vmem_limit_bytes=48 * 2**20
+            collective_id=0, has_side_effects=True, vmem_limit_bytes=60 * 2**20
         ),
         name="layer",
     )(
-        local,
-        qf,
-        qb,
-        state,
-        aux,
-        doc_column,
+        queries,
+        key_rows,
+        value_rows,
         out_gate,
+        log_decay,
+        doc_ids[None, :],
         head_gain[None, :],
         out_weight,
         residual,
-        norm_gain.reshape(2, n_tp, 1, own_width),
-        norm_bias.reshape(2, n_tp, 1, own_width),
+        norm_gain,
+        norm_bias,
         gate_weight,
         up_weight,
         down_weight,

time: 132 us -> 111 us (0.84)
  local copies, waits for them, and re-layouts: 11.9 us -> 1.67 us
  Pallas kernels: 119 us -> 109 us
    unnamed x23 -> x1, local copies, waits for them, and re-layouts: 10.2 us -> 1.67 us
    pallas_call x1, Pallas kernels: 117 us -> 109 us  [on_device(): pl.pallas_call(functools.partial(layer_kernel, sizes), out_shape=jax.Shap...]
    pallas_call x1 -> x0, Pallas kernels: 1.9 us -> none  [on_device(): pl.pallas_call(attend_kernel, out_shape=(jax.ShapeDtypeStruct((length, va...]
    reshape x2 -> x0, local copies, waits for them, and re-layouts: 1.49 us -> none  [the longest x1 0.75 us: on_device(): norm_bias.reshape(2, n_tp, 1, own_width)]
where the time goes in v2:
time: 111 us
  Pallas kernels  109 us (98%)
  local copies, waits for them, and re-layouts  1.67 us (2%)
    pallas_call x1, Pallas kernels, on_device(): pl.pallas_call(functools.partial(layer_kernel, sizes), out_shape=jax.Shap...  109 us

profile of v2, /device:TPU:0, one launch (start us, length us, event | category | flops | bytes accessed | tf_op | source)
XLA Modules:
  0.0 110.7 jit_solution(7375243698787640511)
XLA Ops:
  0.0 109.0 %layer.1 = bf16[256,512]{1,0:T(8,128)(2,1)} custom-call(bf16[256,128]{1,0:T(8,128)(2,1)} %refs_0_.1, bf16[256,128]{1,0:T(8,128)(2,1)} %refs_1_.1, bf16[256,256]{1,0:T(8,128)(2,1)} %refs_2_.1, bf16[256,256]{1,0:T(8,128)(2,1)} %refs_3_.1, f32[2,256,128]{2,1,0:T(8,128)} %refs_4_.1, s32[1,256]{1,0:T(1,128)} %bitcast.2, f32[1,256]{1,0:T(1,128)} %bitcast.3, ...), custom_call_target="tpu_custom_call" | custom-call | tf_op jit(solution)/shard_map/layer/pallas_call | solution.py:448
  109.0 1.7 %copy.16 = bf16[256,512]{1,0:T(8,128)(2,1)} copy(bf16[256,512]{1,0:T(8,128)(2,1)} %layer.1) | data formatting | bytes 524288

commit v3 on v2

--- a/solution.py
+++ b/solution.py
@@ -243,6 +243,7 @@
         return copies
 
     start_own(0)
+    start_own(1)
     for load in loads[:5]:
         load.wait()
     doc_row = docrow_ref[...]
@@ -259,7 +260,7 @@
             copy.start()
             small.append(copy)
 
-    for p in range(1, len(pieces)):
+    for p in range(2, len(pieces)):
         start_own(p)
     for copy in own_copies:
         copy.start()
@@ -301,19 +302,19 @@
         sendbuf[i] = dot(mixed, outweight_ref[:, i * own_width : (i + 1) * own_width]).astype(BF16)
 
     def norm(stream, kind):
-        ones = jnp.ones((8, own_width), F32)
-        sums = dot(ones, stream, ((1,), (1,)), HIGH)
-        squares = dot(ones, stream * stream, ((1,), (1,)), HIGH)
-        moments[kind] = jnp.where(iota((8, length), 0) == 0, sums, squares)
+        def as_row(x):
+            return jnp.sum(jnp.where(eye, jnp.sum(x, axis=1, keepdims=True), 0.0), axis=0, keepdims=True)
+
+        moments[kind] = jnp.where(iota((8, length), 0) == 0, as_row(stream), as_row(stream * stream))
         copies = to_tp(2 + kind, lambda to: moments.at[kind], lambda d: moments_in.at[kind, d - 1])
         for copy in copies:
             copy.wait_recv()
         total = moments[kind]
         for d in range(1, n_tp):
             total = total + moments_in[kind, d - 1]
-        total = dot(jnp.where(eye, 1.0, 0.0), total, ((1,), (1,)), HIGH) / full_width
-        middle = total[:, 0:1]
-        spread = total[:, 1:2] - middle * middle
+        total = total / full_width
+        middle = jnp.sum(jnp.where(eye, total[0:1], 0.0), axis=1, keepdims=True)
+        spread = jnp.sum(jnp.where(eye, total[1:2], 0.0), axis=1, keepdims=True) - middle * middle
         return (stream - middle) * lax.rsqrt(spread + EPS) * gain_ref[kind : kind + 1] + bias_ref[kind : kind + 1]
 
     copies = to_tp(0, lambda to: sendbuf.at[to], lambda d: landed.at[d - 1])

time: 111 us -> 109 us (0.982)
  Pallas kernels: 109 us -> 107 us
    pallas_call x1, Pallas kernels: 109 us -> 107 us  [on_device(): pl.pallas_call(functools.partial(layer_kernel, sizes), out_shape=jax.Shap...]
where the time goes in v3:
time: 109 us
  Pallas kernels  107 us (98%)
  local copies, waits for them, and re-layouts  1.67 us (2%)
    pallas_call x1, Pallas kernels, on_device(): pl.pallas_call(functools.partial(layer_kernel, sizes), out_shape=jax.Shap...  107 us

profile of v3, /device:TPU:0, one launch (start us, length us, event | category | flops | bytes accessed | tf_op | source)
XLA Modules:
  0.0 109.1 jit_solution(18250575606119747410)
XLA Ops:
  0.0 107.5 %layer.1 = bf16[256,512]{1,0:T(8,128)(2,1)} custom-call(bf16[256,128]{1,0:T(8,128)(2,1)} %refs_0_.1, bf16[256,128]{1,0:T(8,128)(2,1)} %refs_1_.1, bf16[256,256]{1,0:T(8,128)(2,1)} %refs_2_.1, bf16[256,256]{1,0:T(8,128)(2,1)} %refs_3_.1, f32[2,256,128]{2,1,0:T(8,128)} %refs_4_.1, s32[1,256]{1,0:T(1,128)} %bitcast.2, f32[1,256]{1,0:T(1,128)} %bitcast.3, ...), custom_call_target="tpu_custom_call" | custom-call | tf_op jit(solution)/shard_map/layer/pallas_call | solution.py:449
  107.5 1.7 %copy.16 = bf16[256,512]{1,0:T(8,128)(2,1)} copy(bf16[256,512]{1,0:T(8,128)(2,1)} %layer.1) | data formatting | bytes 524288
